TPU v7x, 32 devices: a whole 2x2x4 slice. The times are simulated.
32 devices in a mesh: grp: 2 (over x), tp: 4 (over y, core), dp: 4 (over z).
Axes of the slice: x: 2, y: 2, z: 4, core: 2. Of those that a mesh axis runs over, the one named last changes fastest.
Arguments:
- tokens: bfloat16 [512, 2048], P(('grp', 'tp'), 'dp'), parts along dimension 0, may hold values from -25 to 25
- state: float32 [2, 512, 16, 128, 128], P(None, ('grp', 'dp'), 'tp'), parts along dimension 1, may hold values from -1 to 1
- lengths: int32 [512], P(('grp', 'dp')), parts along dimension 0, may hold values from 1 to 4096, 131072 in all
- norm_gain: bfloat16 [2, 2048], P(None, 'dp'), may hold values from 0.099609375 to 1.8984375
- w_query: bfloat16 [2, 2048, 2048], P(None, 'dp', 'tp'), may hold values from -0.125 to 0.125
- w_forget: bfloat16 [2, 2048, 2048], P(None, 'dp', 'tp'), may hold values from -0.125 to 0.125
- w_input: bfloat16 [2, 2048, 2048], P(None, 'dp', 'tp'), may hold values from -0.125 to 0.125
- w_gate: bfloat16 [2, 2048, 2048], P(None, 'dp', 'tp'), may hold values from -0.125 to 0.125
- w_out: bfloat16 [2, 2048, 2048], P(None, 'tp', 'dp'), may hold values from -0.125 to 0.125
- bound_logit: float32 [2, 2048], P(None, 'tp'), may hold values from -3 to 5
- pace: float32 [2, 2048], P(None, 'tp'), may hold values from 0.6 to 2
- head_gain: float32 [2, 128], replicated, may hold values from 0.4 to 2.5
Outputs:
- mixed: float32 [512, 2048], P(('grp', 'tp'), 'dp'), parts along dimension 0
- new_state: float32 [2, 512, 16, 128, 128], P(None, ('grp', 'dp'), 'tp'), parts along dimension 1
There are 2 independent parts, one for each index of `grp`. A program takes and returns all parts, laid end to end along the dimension named above; an argument that names none is the same for every part. Nothing has to cross between parts.
All inputs are finite; a program needn't handle non-finite values. No bound on the sum of `lengths` on one device may be relied on, other than what follows from the above.
Results may differ from a plain program's by a relative error of at most 0.0083.
Values may be sent and summed in bfloat16 or wider, within the bound.
A program may use at most 192 MiB of HBM per device.

v0:
```python
import functools

import jax
import jax.numpy as jnp
from jax import lax
from jax.experimental import pallas as pl
from jax.experimental.pallas import tpu as pltpu
from jax.sharding import PartitionSpec as P

LENGTH_MEAN = 512
epsilon = 1e-06
GROUP = 8
LIMIT = 26 * 1024 * 1024
MESH_ID = pl.DeviceIdType.MESH
f32 = jnp.float32
bf16 = jnp.bfloat16


def chain(
    n_tp,
    n_dp,
    width,
    tokens,
    state,
    lengths,
    gain,
    w_query,
    w_forget,
    w_input,
    w_gate,
    w_out,
    bound,
    pace,
    head_gain,
    mixed,
    sbuf,
    forget_o,
    key_o,
    value_o,
    xall,
    wbuf,
    wobuf,
    psend,
    precv,
    pown,
    nall,
    osend,
    orecv,
    oown,
    gate_s,
    qf_s,
    qk_s,
    ro_s,
    w_sem,
    s_sem,
    x_ss,
    x_rs,
    p_ss,
    p_rs,
    n_ss,
    n_rs,
    o_ss,
    o_rs,
):
    t, d = lax.axis_index("tp"), lax.axis_index("dp")
    rt, feats = tokens.shape
    own, heads, size = state.shape[1], state.shape[2], state.shape[3]
    chans = heads * size
    groups = own // GROUP

    def tp_peer(k):
        return lax.rem(t + k, n_tp)

    def dp_peer(k):
        return lax.rem(d + k, n_dp)

    loads = []
    for b in range(2):
        per = []
        for i, w in enumerate((w_query, w_forget, w_input, w_gate)):
            per.append(pltpu.make_async_copy(w.at[b], wbuf.at[b, i], w_sem.at[b, i]))
        per.append(pltpu.make_async_copy(w_out.at[b], wobuf.at[b], w_sem.at[b, 4]))
        loads.append(per)

    def state_load(b, g):
        rows = pl.ds(g * GROUP, GROUP)
        return pltpu.make_async_copy(state.at[b, rows], sbuf.at[b, rows], s_sem.at[b, g])

    for c in loads[0]:
        c.start()

    barrier = pltpu.get_barrier_semaphore()
    for k in range(1, n_tp):
        pl.semaphore_signal(barrier, inc=1, device_id={"tp": tp_peer(k)}, device_id_type=MESH_ID)
    for k in range(1, n_dp):
        pl.semaphore_signal(barrier, inc=1, device_id={"dp": dp_peer(k)}, device_id_type=MESH_ID)
    pl.semaphore_wait(barrier, n_tp + n_dp - 2)

    my_rows = pl.ds(pl.multiple_of(t * rt, rt), rt)
    my_seqs = pl.ds(pl.multiple_of(d * own, own), own)
    sends = []
    current = tokens[...].astype(f32)
    log_len = jnp.log(lengths[...].astype(f32) / LENGTH_MEAN)
    lane = lax.broadcasted_iota(jnp.int32, (own, 128), 1)
    row_id = lax.broadcasted_iota(jnp.int32, (GROUP, size), 0)

    def advance(b, g, carry):
        rows = pl.ds(pl.multiple_of(g * GROUP, GROUP), GROUP)
        for h in range(heads):
            cols = slice(h * size, (h + 1) * size)
            f_t = forget_o[b, rows, cols].T
            k_t = key_o[b, rows, cols].T
            v = value_o[b, rows, cols]
            for j in range(GROUP):
                at = g * GROUP + j
                sbuf[b, at, h] = f_t[:, j : j + 1] * sbuf[b, at, h] + k_t[:, j : j + 1] * v[j : j + 1, :]
        return carry

    for b in range(2):
        copies = []
        for k in range(1, n_tp):
            c = pltpu.make_async_remote_copy(
                src_ref=tokens if b == 0 else xall.at[b, my_rows],
                dst_ref=xall.at[b, my_rows],
                send_sem=x_ss.at[b, k - 1],
                recv_sem=x_rs.at[b, k - 1],
                device_id={"tp": tp_peer(k)},
                device_id_type=MESH_ID,
            )
            c.start()
            copies.append(c)
        sends += copies
        if b == 0:
            xall[b, my_rows, :] = tokens[...]
            for g in range(groups):
                state_load(0, g).start()
            for c in loads[1]:
                c.start()
            for g in range(groups):
                state_load(1, g).start()
        for i in range(4):
            loads[b][i].wait()
        for c in copies:
            c.wait_recv()

        gain_row = gain[b : b + 1, :].astype(f32)
        copies = []
        for k in [n_dp // 2] + [k for k in range(1, n_dp) if k != n_dp // 2] + [0]:
            dest = dp_peer(k)
            x = xall[b, pl.ds(pl.multiple_of(dest * own, own), own), :].astype(f32)
            sq = jnp.sum(x * x, axis=1, keepdims=True)
            gained = (x * gain_row).astype(bf16)
            for i in range(4):
                part = jnp.dot(gained, wbuf[b, i], preferred_element_type=f32)
                if k == 0:
                    pown[:, i * chans : (i + 1) * chans] = part
                else:
                    psend[b, k - 1, :, i * chans : (i + 1) * chans] = part.astype(bf16)
            if k == 0:
                own_sq = sq
            else:
                hi = sq.astype(bf16).astype(f32)
                packed = jnp.where(lane == 0, hi, jnp.where(lane == 1, sq - hi, 0.0))
                psend[b, k - 1, :, 4 * chans :] = packed.astype(bf16)
                c = pltpu.make_async_remote_copy(
                    src_ref=psend.at[b, k - 1],
                    dst_ref=precv.at[b, k - 1],
                    send_sem=p_ss.at[b, k - 1],
                    recv_sem=p_rs.at[b, k - 1],
                    device_id={"dp": dest},
                    device_id_type=MESH_ID,
                )
                c.start()
                copies.append(c)
        sends += copies
        if b == 1:
            lax.fori_loop(0, groups, functools.partial(advance, 0), 0)
        for c in copies:
            c.wait_recv()

        squares = own_sq
        for k in range(n_dp - 1):
            squares = squares + jnp.sum(precv[b, k, :, 4 * chans :].astype(f32), axis=1, keepdims=True)
        scale = lax.rsqrt(squares / width + epsilon)

        def total(i):
            cols = slice(i * chans, (i + 1) * chans)
            acc = pown[:, cols]
            for k in range(n_dp - 1):
                acc = acc + precv[b, k, :, cols].astype(f32)
            return scale * acc

        lower = jax.nn.sigmoid(bound[b : b + 1, :])
        pre = total(1) - pace[b : b + 1, :] * log_len
        forget = lower + (1.0 - lower) * jax.nn.sigmoid(pre)
        key = (1.0 - lower) * jax.nn.sigmoid(-pre)
        forget_o[b] = forget
        key_o[b] = key
        query = total(0)
        qf_s[...] = query * forget
        qk_s[...] = query * key
        value_o[b] = total(2)
        gate = total(3)
        gate_s[...] = gate * jax.nn.sigmoid(gate)

        for g in range(groups):
            state_load(b, g).wait()

        def read(g, carry):
            rows = pl.ds(pl.multiple_of(g * GROUP, GROUP), GROUP)
            for h in range(heads):
                cols = slice(h * size, (h + 1) * size)
                q8 = qf_s[rows, cols]
                diag = jnp.concatenate(
                    [jnp.where(row_id == j, q8, 0.0) for j in range(GROUP)], axis=1
                ).astype(bf16)
                s8 = sbuf[b, rows, h].reshape(GROUP * size, size).astype(bf16)
                ro_s[rows, cols] = jnp.dot(diag, s8, preferred_element_type=f32)
            return carry

        lax.fori_loop(0, groups, read, 0)
        for h in range(heads):
            cols = slice(h * size, (h + 1) * size)
            dots = jnp.sum(qk_s[:, cols], axis=1, keepdims=True)
            readout = ro_s[:, cols] + dots * value_o[b, :, cols]
            mean = jnp.mean(readout * readout, axis=1, keepdims=True)
            normed = readout * lax.rsqrt(mean + epsilon) * head_gain[b : b + 1, :] * gate_s[:, cols]
            nall[b, my_seqs, cols] = normed.astype(bf16)

        copies = []
        for k in range(1, n_dp):
            c = pltpu.make_async_remote_copy(
                src_ref=nall.at[b, my_seqs],
                dst_ref=nall.at[b, my_seqs],
                send_sem=n_ss.at[b, k - 1],
                recv_sem=n_rs.at[b, k - 1],
                device_id={"dp": dp_peer(k)},
                device_id_type=MESH_ID,
            )
            c.start()
            copies.append(c)
        sends += copies
        loads[b][4].wait()
        if b == 1:
            lax.fori_loop(0, groups, functools.partial(advance, 1), 0)
        for c in copies:
            c.wait_recv()

        copies = []
        for k in list(range(1, n_tp)) + [0]:
            dest = tp_peer(k)
            rows = nall[b, pl.ds(pl.multiple_of(dest * rt, rt), rt), :]
            part = jnp.dot(rows, wobuf[b], preferred_element_type=f32)
            if k == 0:
                oown[...] = part
            else:
                osend[b, k - 1] = part.astype(bf16)
                c = pltpu.make_async_remote_copy(
                    src_ref=osend.at[b, k - 1],
                    dst_ref=orecv.at[b, k - 1],
                    send_sem=o_ss.at[b, k - 1],
                    recv_sem=o_rs.at[b, k - 1],
                    device_id={"tp": dest},
                    device_id_type=MESH_ID,
                )
                c.start()
                copies.append(c)
        sends += copies
        for c in copies:
            c.wait_recv()
        branch = oown[...]
        for k in range(n_tp - 1):
            branch = branch + orecv[b, k].astype(f32)
        if b == 0:
            rounded = (current + branch).astype(bf16)
            xall[1, my_rows, :] = rounded
            current = rounded.astype(f32)
        else:
            mixed[...] = current + branch

    for c in sends:
        c.wait_send()


def store(mixed, new_state, mixed_out, state_out, sems):
    blocks, own = new_state.shape[:2]
    copies = [pltpu.make_async_copy(mixed, mixed_out, sems.at[blocks, 0])]
    for b in range(blocks):
        for g in range(own // GROUP):
            rows = pl.ds(g * GROUP, GROUP)
            copies.append(pltpu.make_async_copy(new_state.at[b, rows], state_out.at[b, rows], sems.at[b, g]))
    for c in copies:
        c.start()
    for c in copies:
        c.wait()


def shards(n_tp, n_dp, tokens, state, lengths, gain, w_query, w_forget, w_input, w_gate, w_out, bound, pace, head_gain):
    rt, feats = tokens.shape
    own, heads, size = state.shape[1:4]
    chans = heads * size
    rows = rt * n_tp
    msg = 4 * chans + 128
    vmem = pl.BlockSpec(memory_space=pltpu.VMEM)
    hbm = pl.BlockSpec(memory_space=pl.ANY)
    gates = pltpu.VMEM((2, own, chans), f32)
    dma = pltpu.SemaphoreType.DMA
    mixed, new_state = pl.pallas_call(
        functools.partial(chain, n_tp, n_dp, feats * n_dp),
        name="chain",
        out_shape=(pltpu.VMEM((rt, feats), f32), pltpu.VMEM(state.shape, f32)),
        in_specs=[vmem, hbm, vmem, vmem] + [hbm] * 5 + [vmem] * 3,
        out_specs=(vmem, vmem),
        scratch_shapes=[
            gates,
            gates,
            gates,
            pltpu.VMEM((2, rows, feats), bf16),
            pltpu.VMEM((2, 4, feats, chans), bf16),
            pltpu.VMEM((2, chans, feats), bf16),
            pltpu.VMEM((2, n_dp - 1, own, msg), bf16),
            pltpu.VMEM((2, n_dp - 1, own, msg), bf16),
            pltpu.VMEM((own, 4 * chans), f32),
            pltpu.VMEM((2, rows, chans), bf16),
            pltpu.VMEM((2, n_tp - 1, rt, feats), bf16),
            pltpu.VMEM((2, n_tp - 1, rt, feats), bf16),
            pltpu.VMEM((rt, feats), f32),
            pltpu.VMEM((own, chans), f32),
            pltpu.VMEM((own, chans), f32),
            pltpu.VMEM((own, chans), f32),
            pltpu.VMEM((own, chans), f32),
            dma((2, 5)),
            dma((2, own // GROUP)),
            dma((2, n_tp - 1)),
            dma((2, n_tp - 1)),
            dma((2, n_dp - 1)),
            dma((2, n_dp - 1)),
            dma((2, n_dp - 1)),
            dma((2, n_dp - 1)),
            dma((2, n_tp - 1)),
            dma((2, n_tp - 1)),
        ],
        compiler_params=pltpu.CompilerParams(
            collective_id=0, has_side_effects=True, vmem_limit_bytes=LIMIT
        ),
    )(tokens, state, lengths[:, None], gain, w_query, w_forget, w_input, w_gate, w_out, bound, pace, head_gain)

    return pl.pallas_call(
        store,
        name="store",
        out_shape=(jax.ShapeDtypeStruct((rt, feats), f32), jax.ShapeDtypeStruct(state.shape, f32)),
        in_specs=[vmem, vmem],
        out_specs=(hbm, hbm),
        scratch_shapes=[dma((3, own // GROUP))],
        compiler_params=pltpu.CompilerParams(vmem_limit_bytes=LIMIT),
    )(pltpu.with_memory_space_constraint(mixed, pltpu.VMEM), pltpu.with_memory_space_constraint(new_state, pltpu.VMEM))


def solution(mesh):
    in_specs = (
        P(("grp", "tp"), "dp"),
        P(None, ("grp", "dp"), "tp", None, None),
        P(("grp", "dp")),
        P(None, "dp"),
        P(None, "dp", "tp"),
        P(None, "dp", "tp"),
        P(None, "dp", "tp"),
        P(None, "dp", "tp"),
        P(None, "tp", "dp"),
        P(None, "tp"),
        P(None, "tp"),
        P(),
    )
    out_specs = (P(("grp", "tp"), "dp"), P(None, ("grp", "dp"), "tp", None, None))
    body = functools.partial(shards, mesh.shape["tp"], mesh.shape["dp"])
    return jax.shard_map(body, mesh=mesh, in_specs=in_specs, out_specs=out_specs, check_vma=False)
```

profile of v0, /device:TPU:23, one launch (start us, length us, event | category | flops | bytes accessed | tf_op | source)
XLA Modules:
  0.0 108.8 jit_solution(16102932543065235536)
XLA Ops:
  0.6 1.4 %copy.14.lengths = s32[64,1]{1,0:T(8,128)} copy(s32[64,1]{0,1:T(1,128)} %bitcast.1) | data formatting | bytes 512 | tf_op jit(solution)/shard_map/broadcast_in_dim | solution.py:346
  2.0 95.7 %chain.1 = (f32[64,512]{1,0:T(8,128)S(1)}, f32[2,64,4,128,128]{4,3,2,1,0:T(8,128)S(1)}) custom-call(bf16[64,512]{1,0:T(8,128)(2,1)} %tokens.1, f32[2,64,4,128,128]{4,3,2,1,0:T(8,128)} %state.1, s32[64,1]{1,0:T(8,128)} %copy.14.lengths, bf16[2,512]{1,0:T(2,128)(2,1)} %gain.1, bf16[2,512,512]{2,1,0:T(8,128)(2,1)} %w_query.1, bf16[2,512,512]{2,1,0:T(8,128)(2,1)} %w_forget.1, ...), custom_call_target="tpu_custom_call" | custom-call | tf_op jit(solution)/shard_map/chain/pallas_call | solution.py:308
  97.7 11.2 %store.1 = (f32[64,512]{1,0:T(8,128)}, f32[2,64,4,128,128]{4,3,2,1,0:T(8,128)}) custom-call(f32[64,512]{1,0:T(8,128)S(1)} %get-tuple-element.4.mixed, f32[2,64,4,128,128]{4,3,2,1,0:T(8,128)S(1)} %get-tuple-element.5.new_state), custom_call_target="tpu_custom_call" | custom-call | tf_op jit(solution)/shard_map/store/pallas_call | solution.py:348
where the time goes:
time: 109 us
  Pallas kernels  107 us (98%)
  local copies, waits for them, and re-layouts  1.36 us (1%)
    pallas_call x1, Pallas kernels, shards(): pl.pallas_call(functools.partial(chain, n_tp, n_dp, feats * n_dp), name='...  95.7 us
    pallas_call x1, Pallas kernels, shards(): pl.pallas_call(store, name='store', out_shape=(jax.ShapeDtypeStruct((rt,...  11.2 us

commit v1 on v0

v1 whole, which is shorter than its diff:
```python
import functools

import jax
import jax.numpy as jnp
from jax import lax
from jax.experimental import pallas as pl
from jax.experimental.pallas import tpu as pltpu
from jax.sharding import PartitionSpec as P

LENGTH_MEAN = 512
epsilon = 1e-06
GROUP = 8
LIMIT = 26 * 1024 * 1024
MESH_ID = pl.DeviceIdType.MESH
f32 = jnp.float32
bf16 = jnp.bfloat16


def chain(
    n_tp,
    n_dp,
    width,
    parts,
    tokens,
    state,
    lengths,
    gain,
    w_query,
    w_forget,
    w_input,
    w_gate,
    w_out,
    bound,
    pace,
    head_gain,
    mixed,
    sbuf,
    lengths_s,
    gain_s,
    bound_s,
    pace_s,
    hgain_s,
    forget_s,
    value_s,
    xall,
    wbuf,
    wobuf,
    pf,
    sq_s,
    psend,
    precv,
    relay,
    nall,
    po,
    osend,
    orecv,
    gate_s,
    qf_s,
    qk_s,
    ro_s,
    in_sem,
    t_sem,
    w_sem,
    s_sem,
    x_ss,
    x_rs,
    p_ss,
    p_rs,
    r_rs,
    n_ss,
    n_rs,
    o_ss,
    o_rs,
):
    t, d = lax.axis_index("tp"), lax.axis_index("dp")
    rt, feats = tokens.shape
    own, heads, size = state.shape[1], state.shape[2], state.shape[3]
    chans = heads * size
    hr, rh = own // parts, rt // parts
    rows_all = n_dp * hr
    per_part = hr // GROUP
    relayed = n_dp >= 4
    last = n_dp - 2
    at_end = jnp.logical_or(d == 0, d == n_dp - 1)
    merging = jnp.logical_or(d == 1, d == n_dp - 2)

    def tp_peer(k):
        return lax.rem(t + k, n_tp)

    def dp_peer(k):
        return lax.rem(d + k, n_dp)

    def start_all(copies):
        for c in copies:
            c.start()

    token_loads = [
        pltpu.make_async_copy(tokens.at[pl.ds(p * rh, rh)], xall.at[0, p, t], t_sem.at[p]) for p in range(parts)
    ]
    small = [
        pltpu.make_async_copy(src, dst, in_sem.at[i])
        for i, (src, dst) in enumerate(
            ((gain, gain_s), (lengths, lengths_s), (bound, bound_s), (pace, pace_s), (head_gain, hgain_s))
        )
    ]
    loads = []
    for b in range(2):
        per = []
        for i, w in enumerate((w_query, w_forget, w_input, w_gate)):
            per.append(pltpu.make_async_copy(w.at[b], wbuf.at[b, i], w_sem.at[b, i]))
        per.append(pltpu.make_async_copy(w_out.at[b], wobuf.at[b], w_sem.at[b, 4]))
        loads.append(per)

    def state_load(b, g):
        rows = pl.ds(g * GROUP, GROUP)
        return pltpu.make_async_copy(state.at[b, rows], sbuf.at[b, rows], s_sem.at[b, g])

    start_all(token_loads)
    start_all(small)
    start_all(loads[0])

    barrier = pltpu.get_barrier_semaphore()
    for k in range(1, n_tp):
        pl.semaphore_signal(barrier, inc=1, device_id={"tp": tp_peer(k)}, device_id_type=MESH_ID)
    for k in range(1, n_dp):
        pl.semaphore_signal(barrier, inc=1, device_id={"dp": dp_peer(k)}, device_id_type=MESH_ID)
    pl.semaphore_wait(barrier, n_tp + n_dp - 2)

    sends = []
    lane = lax.broadcasted_iota(jnp.int32, (hr, 128), 1)
    row_id = lax.broadcasted_iota(jnp.int32, (GROUP, size), 0)
    spread = jnp.where(
        lax.broadcasted_iota(jnp.int32, (GROUP, GROUP * size), 1) // size
        == lax.broadcasted_iota(jnp.int32, (GROUP, GROUP * size), 0),
        1.0,
        0.0,
    ).astype(bf16)
    spread = jnp.concatenate([spread] * 3, axis=0)

    def far_first(n):
        return [n // 2] + [k for k in range(1, n) if k != n // 2]

    def x_copy(b, p, k):
        return pltpu.make_async_remote_copy(
            src_ref=xall.at[b, p, t],
            dst_ref=xall.at[b, p, t],
            send_sem=x_ss.at[b, p, k - 1],
            recv_sem=x_rs.at[b, p, k - 1],
            device_id={"tp": tp_peer(k)},
            device_id_type=MESH_ID,
        )

    def share(b, p):
        for k in far_first(n_tp):
            c = x_copy(b, p, k)
            c.start()
            sends.append(c)

    def offset(i):
        if not relayed:
            return far_first(n_dp)[i]
        if i == last:
            middle = jnp.where(d == 1, n_dp - 2, jnp.where(d == n_dp - 2, 2, n_dp - 1))
        else:
            skip = jnp.where(d == 1, n_dp - 2, jnp.where(d == n_dp - 2, 2, n_dp - 1))
            middle = jnp.where(i + 1 < skip, i + 1, i + 2)
        return jnp.where(d == 0, n_dp - 1 - i, jnp.where(d == n_dp - 1, i + 1, middle))

    def partial_copy(b, p, k):
        dest = dp_peer(k)
        return pltpu.make_async_remote_copy(
            src_ref=psend.at[b, p, dest],
            dst_ref=precv.at[b, p, k - 1],
            send_sem=p_ss.at[b, p, k - 1],
            recv_sem=p_rs.at[b, p, k - 1],
            device_id={"dp": dest},
            device_id_type=MESH_ID,
        )

    def relay_copy(b, p, k):
        return pltpu.make_async_remote_copy(
            src_ref=psend.at[b, p, dp_peer(k)],
            dst_ref=relay.at[b, p],
            send_sem=p_ss.at[b, p, k - 1],
            recv_sem=r_rs.at[b, p],
            device_id={"dp": jnp.where(d == 0, 1, n_dp - 2)},
            device_id_type=MESH_ID,
        )

    def pack(sq):
        hi = sq.astype(bf16).astype(f32)
        return jnp.where(lane == 0, hi, jnp.where(lane == 1, sq - hi, 0.0)).astype(bf16)

    def send_step(b, p, i):
        k = offset(i)
        c = partial_copy(b, p, k)
        if relayed and i == 0:

            @pl.when(at_end)
            def _():
                relay_copy(b, p, k).start()

            @pl.when(jnp.logical_not(at_end))
            def _():
                c.start()

        else:
            if relayed and i == last:

                @pl.when(merging)
                def _():
                    relay_copy(b, p, k).wait_recv()
                    dest = dp_peer(k)
                    for j in range(4):
                        cols = slice(j * chans, (j + 1) * chans)
                        both = pf[p, dest, :, cols] + relay[b, p, :, cols].astype(f32)
                        psend[b, p, dest, :, cols] = both.astype(bf16)
                    far = jnp.sum(relay[b, p, :, 4 * chans :].astype(f32), axis=1, keepdims=True)
                    psend[b, p, dest, :, 4 * chans :] = pack(sq_s[p, dest] + far)

            c.start()
        sends.append(c)

    def project(b, p):
        if p == 0:
            for i in range(4):
                loads[b][i].wait()
        for k in range(1, n_tp):
            x_copy(b, p, k).wait_recv()
        x = xall[b, p].reshape(rows_all, feats).astype(f32)
        sq = jnp.sum(x * x, axis=1, keepdims=True)
        gained = (x * gain_s[b : b + 1, :].astype(f32)).astype(bf16)
        sq_s[p] = jnp.broadcast_to(sq, (rows_all, 128)).reshape(n_dp, hr, 128)
        for e in range(n_dp):
            psend[b, p, e, :, 4 * chans :] = pack(jnp.broadcast_to(sq[e * hr : (e + 1) * hr], (hr, 128)))
        for i in range(4):
            cols = slice(i * chans, (i + 1) * chans)
            part = jnp.dot(gained, wbuf[b, i], preferred_element_type=f32)
            pf[p, :, :, cols] = part.reshape(n_dp, hr, chans)
            psend[b, p, :, :, cols] = part.astype(bf16).reshape(n_dp, hr, chans)
        for i in range(last):
            send_step(b, p, i)

    def finish_sends(b, p):
        send_step(b, p, last)

    def gates(b, p):
        if b == 0 and p == 0:
            for c in small[1:]:
                c.wait()
        for k in range(1, n_dp):
            c = partial_copy(b, p, k)
            if relayed and k == 1:
                pl.when(d != 0)(c.wait_recv)
            elif relayed and k == n_dp - 1:
                pl.when(d != n_dp - 1)(c.wait_recv)
            else:
                c.wait_recv()

        squares = sq_s[p, d, :, :1]
        for k in range(n_dp - 1):
            squares = squares + jnp.sum(precv[b, p, k, :, 4 * chans :].astype(f32), axis=1, keepdims=True)
        scale = lax.rsqrt(squares / width + epsilon)

        def total(i):
            cols = slice(i * chans, (i + 1) * chans)
            acc = pf[p, d, :, cols]
            for k in range(n_dp - 1):
                acc = acc + precv[b, p, k, :, cols].astype(f32)
            return scale * acc

        rows = slice(p * hr, (p + 1) * hr)
        log_row = jnp.log(lengths_s[...].astype(f32) / LENGTH_MEAN)
        pick = lax.broadcasted_iota(jnp.int32, (hr, own), 1) == lax.broadcasted_iota(jnp.int32, (hr, own), 0) + p * hr
        log_len = jnp.sum(jnp.where(pick, log_row, 0.0), axis=1, keepdims=True)
        lower = jax.nn.sigmoid(bound_s[b : b + 1, :])
        pre = total(1) - pace_s[b : b + 1, :] * log_len
        forget = lower + (1.0 - lower) * jax.nn.sigmoid(pre)
        key = (1.0 - lower) * jax.nn.sigmoid(-pre)
        forget_s[b, rows] = forget
        query = total(0)
        qf_s[...] = query * forget
        qk_s[...] = query * key
        value_s[b, rows] = total(2)
        gate = total(3)
        gate_s[...] = gate * jax.nn.sigmoid(gate)

        for g in range(per_part):
            state_load(b, p * per_part + g).wait()

        def read(g, carry):
            at = pl.ds(pl.multiple_of(g * GROUP, GROUP), GROUP)
            seqs = pl.ds(pl.multiple_of(p * hr + g * GROUP, GROUP), GROUP)
            for h in range(heads):
                cols = slice(h * size, (h + 1) * size)
                q8 = qf_s[at, cols]
                diag = jnp.concatenate(
                    [jnp.where(row_id == j, q8, 0.0) for j in range(GROUP)], axis=1
                ).astype(bf16)
                s8 = sbuf[b, seqs, h].reshape(GROUP * size, size).astype(bf16)
                ro_s[at, cols] = jnp.dot(diag, s8, preferred_element_type=f32)
            return carry

        lax.fori_loop(0, per_part, read, 0)
        for h in range(heads):
            cols = slice(h * size, (h + 1) * size)
            dots = jnp.sum(qk_s[:, cols], axis=1, keepdims=True)
            readout = ro_s[:, cols] + dots * value_s[b, rows, cols]
            mean = jnp.mean(readout * readout, axis=1, keepdims=True)
            normed = readout * lax.rsqrt(mean + epsilon) * hgain_s[b : b + 1, :] * gate_s[:, cols]
            nall[b, p, d, :, cols] = normed.astype(bf16)
        for k in far_first(n_dp):
            c = normed_copy(b, p, k)
            c.start()
            sends.append(c)

    def normed_copy(b, p, k):
        return pltpu.make_async_remote_copy(
            src_ref=nall.at[b, p, d],
            dst_ref=nall.at[b, p, d],
            send_sem=n_ss.at[b, p, k - 1],
            recv_sem=n_rs.at[b, p, k - 1],
            device_id={"dp": dp_peer(k)},
            device_id_type=MESH_ID,
        )

    def out_copy(b, p, k):
        dest = tp_peer(k)
        return pltpu.make_async_remote_copy(
            src_ref=osend.at[b, p, dest],
            dst_ref=orecv.at[b, p, k - 1],
            send_sem=o_ss.at[b, p, k - 1],
            recv_sem=o_rs.at[b, p, k - 1],
            device_id={"tp": dest},
            device_id_type=MESH_ID,
        )

    def out_project(b, p):
        if p == 0:
            loads[b][4].wait()
        for k in range(1, n_dp):
            normed_copy(b, p, k).wait_recv()
        rows = nall[b, p].reshape(rows_all, chans)
        part = jnp.dot(rows, wobuf[b], preferred_element_type=f32)
        po[p] = part.reshape(n_tp, rh, feats)
        osend[b, p] = part.astype(bf16).reshape(n_tp, rh, feats)
        for k in far_first(n_tp):
            c = out_copy(b, p, k)
            c.start()
            sends.append(c)

    def residual(b, p):
        for k in range(1, n_tp):
            out_copy(b, p, k).wait_recv()
        branch = po[p, t]
        for k in range(n_tp - 1):
            branch = branch + orecv[b, p, k].astype(f32)
        result = xall[b, p, t].astype(f32) + branch
        if b == 0:
            xall[1, p, t] = result.astype(bf16)
            share(1, p)
        else:
            mixed[p * rh : (p + 1) * rh, :] = result

    def advance(b, p):
        def step(g, carry):
            base = pl.multiple_of(p * hr + g * GROUP, GROUP)
            rows = pl.ds(base, GROUP)
            f = forget_s[b, rows, :]
            top = f.astype(bf16)
            rest = f - top.astype(f32)
            mid = rest.astype(bf16)
            low = (rest - mid.astype(f32)).astype(bf16)
            pieces = jnp.concatenate([top, mid, low], axis=0)
            for h in range(heads):
                cols = slice(h * size, (h + 1) * size)
                v = value_s[b, rows, cols]
                for j in range(0, GROUP, 2):
                    wide = lax.dot_general(
                        pieces[:, cols],
                        spread[:, j * size : (j + 2) * size],
                        (((0,), (0,)), ((), ())),
                        preferred_element_type=f32,
                    )
                    for i in range(2):
                        row = v[j + i : j + i + 1, :]
                        keep = wide[:, i * size : (i + 1) * size]
                        sbuf[b, base + j + i, h] = row + keep * (sbuf[b, base + j + i, h] - row)
            return carry

        lax.fori_loop(0, per_part, step, 0)

    if relayed:
        for k, end in ((1, 0), (n_dp - 1, n_dp - 1)):

            @pl.when(d == end)
            def _():
                for b in range(2):
                    for p in range(parts):
                        precv[b, p, k - 1] = jnp.zeros(precv.shape[3:], bf16)

    for p in range(parts):
        token_loads[p].wait()
        share(0, p)
    for g in range(own // GROUP):
        state_load(0, g).start()
    start_all(loads[1])
    for g in range(own // GROUP):
        state_load(1, g).start()
    small[0].wait()

    if parts == 1:
        order = []
        for b in range(2):
            order += [(f, b, 0) for f in (project, finish_sends, gates, advance, out_project, residual)]
    else:
        order = [
            (project, 0, 0),
            (finish_sends, 0, 0),
            (project, 0, 1),
            (gates, 0, 0),
            (finish_sends, 0, 1),
            (advance, 0, 0),
            (out_project, 0, 0),
            (gates, 0, 1),
            (residual, 0, 0),
            (project, 1, 0),
            (advance, 0, 1),
            (out_project, 0, 1),
            (finish_sends, 1, 0),
            (residual, 0, 1),
            (project, 1, 1),
            (gates, 1, 0),
            (finish_sends, 1, 1),
            (advance, 1, 0),
            (out_project, 1, 0),
            (gates, 1, 1),
            (residual, 1, 0),
            (advance, 1, 1),
            (out_project, 1, 1),
            (residual, 1, 1),
        ]
    for f, b, p in order:
        f(b, p)

    for c in sends:
        c.wait_send()


def store(mixed, new_state, mixed_out, state_out, sems):
    blocks, own = new_state.shape[:2]
    copies = [pltpu.make_async_copy(mixed, mixed_out, sems.at[blocks, 0])]
    for b in range(blocks):
        for g in range(own // GROUP):
            rows = pl.ds(g * GROUP, GROUP)
            copies.append(pltpu.make_async_copy(new_state.at[b, rows], state_out.at[b, rows], sems.at[b, g]))
    for c in copies:
        c.start()
    for c in copies:
        c.wait()


def shards(n_tp, n_dp, tokens, state, lengths, gain, w_query, w_forget, w_input, w_gate, w_out, bound, pace, head_gain):
    rt, feats = tokens.shape
    own, heads, size = state.shape[1:4]
    chans = heads * size
    parts = 2 if own == rt and own % (4 * GROUP) == 0 else 1
    hr, rh = own // parts, rt // parts
    msg = 4 * chans + 128
    vmem = pl.BlockSpec(memory_space=pltpu.VMEM)
    hbm = pl.BlockSpec(memory_space=pl.ANY)
    dma = pltpu.SemaphoreType.DMA
    mixed, new_state = pl.pallas_call(
        functools.partial(chain, n_tp, n_dp, feats * n_dp, parts),
        name="chain",
        out_shape=(pltpu.VMEM((rt, feats), f32), pltpu.VMEM(state.shape, f32)),
        in_specs=[hbm] * 12,
        out_specs=(vmem, vmem),
        scratch_shapes=[
            pltpu.VMEM((1, own), jnp.int32),
            pltpu.VMEM(gain.shape, bf16),
            pltpu.VMEM(bound.shape, f32),
            pltpu.VMEM(pace.shape, f32),
            pltpu.VMEM(head_gain.shape, f32),
            pltpu.VMEM((2, own, chans), f32),
            pltpu.VMEM((2, own, chans), f32),
            pltpu.VMEM((2, parts, n_tp, rh, feats), bf16),
            pltpu.VMEM((2, 4, feats, chans), bf16),
            pltpu.VMEM((2, chans, feats), bf16),
            pltpu.VMEM((parts, n_dp, hr, 4 * chans), f32),
            pltpu.VMEM((parts, n_dp, hr, 128), f32),
            pltpu.VMEM((2, parts, n_dp, hr, msg), bf16),
            pltpu.VMEM((2, parts, n_dp - 1, hr, msg), bf16),
            pltpu.VMEM((2, parts, hr, msg), bf16),
            pltpu.VMEM((2, parts, n_dp, hr, chans), bf16),
            pltpu.VMEM((parts, n_tp, rh, feats), f32),
            pltpu.VMEM((2, parts, n_tp, rh, feats), bf16),
            pltpu.VMEM((2, parts, n_tp - 1, rh, feats), bf16),
            pltpu.VMEM((hr, chans), f32),
            pltpu.VMEM((hr, chans), f32),
            pltpu.VMEM((hr, chans), f32),
            pltpu.VMEM((hr, chans), f32),
            dma((5,)),
            dma((parts,)),
            dma((2, 5)),
            dma((2, own // GROUP)),
            dma((2, parts, n_tp - 1)),
            dma((2, parts, n_tp - 1)),
            dma((2, parts, n_dp - 1)),
            dma((2, parts, n_dp - 1)),
            dma((2, parts)),
            dma((2, parts, n_dp - 1)),
            dma((2, parts, n_dp - 1)),
            dma((2, parts, n_tp - 1)),
            dma((2, parts, n_tp - 1)),
        ],
        compiler_params=pltpu.CompilerParams(
            collective_id=0, has_side_effects=True, vmem_limit_bytes=LIMIT
        ),
    )(tokens, state, lengths[None, :], gain, w_query, w_forget, w_input, w_gate, w_out, bound, pace, head_gain)

    return pl.pallas_call(
        store,
        name="store",
        out_shape=(jax.ShapeDtypeStruct((rt, feats), f32), jax.ShapeDtypeStruct(state.shape, f32)),
        in_specs=[vmem, vmem],
        out_specs=(hbm, hbm),
        scratch_shapes=[dma((3, own // GROUP))],
        compiler_params=pltpu.CompilerParams(vmem_limit_bytes=LIMIT),
    )(pltpu.with_memory_space_constraint(mixed, pltpu.VMEM), pltpu.with_memory_space_constraint(new_state, pltpu.VMEM))


def solution(mesh):
    in_specs = (
        P(("grp", "tp"), "dp"),
        P(None, ("grp", "dp"), "tp", None, None),
        P(("grp", "dp")),
        P(None, "dp"),
        P(None, "dp", "tp"),
        P(None, "dp", "tp"),
        P(None, "dp", "tp"),
        P(None, "dp", "tp"),
        P(None, "tp", "dp"),
        P(None, "tp"),
        P(None, "tp"),
        P(),
    )
    out_specs = (P(("grp", "tp"), "dp"), P(None, ("grp", "dp"), "tp", None, None))
    body = functools.partial(shards, mesh.shape["tp"], mesh.shape["dp"])
    return jax.shard_map(body, mesh=mesh, in_specs=in_specs, out_specs=out_specs, check_vma=False)
```

time: 109 us -> 83.7 us (0.77)
  the two profiles are of different devices: /device:TPU:23 before, /device:TPU:0 now
where the time goes in v1:
time: 83.7 us; the launch traced here: 83.5 us
  Pallas kernels  82.9 us (99%)
    pallas_call x1, Pallas kernels, shards(): pl.pallas_call(functools.partial(chain, n_tp, n_dp, feats * n_dp, parts),...  71.8 us
    pallas_call x1, Pallas kernels, shards(): pl.pallas_call(store, name='store', out_shape=(jax.ShapeDtypeStruct((rt,...  11.2 us

profile of v1, /device:TPU:0, one launch (start us, length us, event | category | flops | bytes accessed | tf_op | source)
XLA Modules:
  0.0 83.5 jit_solution(15825979940672085008)
XLA Ops:
  0.6 71.8 %chain.1 = (f32[64,512]{1,0:T(8,128)S(1)}, f32[2,64,4,128,128]{4,3,2,1,0:T(8,128)S(1)}) custom-call(bf16[64,512]{1,0:T(8,128)(2,1)} %tokens.1, f32[2,64,4,128,128]{4,3,2,1,0:T(8,128)} %state.1, s32[1,64]{1,0:T(1,128)} %bitcast.1, bf16[2,512]{1,0:T(2,128)(2,1)} %gain.1, bf16[2,512,512]{2,1,0:T(8,128)(2,1)} %w_query.1, bf16[2,512,512]{2,1,0:T(8,128)(2,1)} %w_forget.1, ...), custom_call_target="tpu_custom_call" | custom-call | tf_op jit(solution)/shard_map/chain/pallas_call | solution.py:473
  72.4 11.2 %store.1 = (f32[64,512]{1,0:T(8,128)}, f32[2,64,4,128,128]{4,3,2,1,0:T(8,128)}) custom-call(f32[64,512]{1,0:T(8,128)S(1)} %get-tuple-element.4.mixed, f32[2,64,4,128,128]{4,3,2,1,0:T(8,128)S(1)} %get-tuple-element.5.new_state), custom_call_target="tpu_custom_call" | custom-call | tf_op jit(solution)/shard_map/store/pallas_call | solution.py:522

commit v2 on v1

--- a/solution.py
+++ b/solution.py
@@ -10,10 +10,21 @@
 LENGTH_MEAN = 512
 epsilon = 1e-06
 GROUP = 8
+PARTS = 4
+RELAYS = 2
 LIMIT = 26 * 1024 * 1024
 MESH_ID = pl.DeviceIdType.MESH
 f32 = jnp.float32
 bf16 = jnp.bfloat16
+
+
+ORDER = (
+    "P0", "P1", "E0", "E1", "M0", "N0", "M1", "N1", "G0", "A0", "P2", "G1", "A1", "P3", "E2", "E3", "O0",
+    "M2", "N2", "M3", "Z0", "N3", "G2", "A2", "O1", "Y0", "P4", "Z1", "G3", "A3", "V3", "O2", "E4", "Y1",
+    "P5", "M4", "E5", "Z2", "O3", "M5", "Z3", "Y2", "N4", "N5", "P6", "Y3", "P7", "E6", "M6", "E7", "N6",
+    "G5", "M7", "V2", "N7", "V1", "G4", "A4", "V0", "A5", "G6", "A6", "G7", "A7", "O4", "O5", "V4", "O6",
+    "O7", "V6", "Y4", "V5", "V7", "Y6", "Y5", "Y7",
+)
 
 
 def chain(
@@ -46,7 +57,7 @@
     wbuf,
     wobuf,
     pf,
-    sq_s,
+    sqx,
     psend,
     precv,
     relay,
@@ -54,6 +65,9 @@
     po,
     osend,
     orecv,
+    pair,
+    zsend,
+    zrecv,
     gate_s,
     qf_s,
     qk_s,
@@ -67,10 +81,16 @@
     p_ss,
     p_rs,
     r_rs,
+    q_ss,
+    q_rs,
     n_ss,
     n_rs,
     o_ss,
     o_rs,
+    d_ss,
+    d_rs,
+    z_ss,
+    z_rs,
 ):
     t, d = lax.axis_index("tp"), lax.axis_index("dp")
     rt, feats = tokens.shape
@@ -80,7 +100,8 @@
     rows_all = n_dp * hr
     per_part = hr // GROUP
     relayed = n_dp >= 4
-    last = n_dp - 2
+    hops = min(RELAYS, n_dp - 2)
+    core, chip, chips = lax.rem(t, 2), lax.div(t, 2), n_tp // 2
     at_end = jnp.logical_or(d == 0, d == n_dp - 1)
     merging = jnp.logical_or(d == 1, d == n_dp - 2)
 
@@ -127,7 +148,6 @@
     pl.semaphore_wait(barrier, n_tp + n_dp - 2)
 
     sends = []
-    lane = lax.broadcasted_iota(jnp.int32, (hr, 128), 1)
     row_id = lax.broadcasted_iota(jnp.int32, (GROUP, size), 0)
     spread = jnp.where(
         lax.broadcasted_iota(jnp.int32, (GROUP, GROUP * size), 1) // size
@@ -156,16 +176,6 @@
             c.start()
             sends.append(c)
 
-    def offset(i):
-        if not relayed:
-            return far_first(n_dp)[i]
-        if i == last:
-            middle = jnp.where(d == 1, n_dp - 2, jnp.where(d == n_dp - 2, 2, n_dp - 1))
-        else:
-            skip = jnp.where(d == 1, n_dp - 2, jnp.where(d == n_dp - 2, 2, n_dp - 1))
-            middle = jnp.where(i + 1 < skip, i + 1, i + 2)
-        return jnp.where(d == 0, n_dp - 1 - i, jnp.where(d == n_dp - 1, i + 1, middle))
-
     def partial_copy(b, p, k):
         dest = dp_peer(k)
         return pltpu.make_async_remote_copy(
@@ -177,72 +187,112 @@
             device_id_type=MESH_ID,
         )
 
-    def relay_copy(b, p, k):
+    def relay_copy(b, p, k, i):
         return pltpu.make_async_remote_copy(
             src_ref=psend.at[b, p, dp_peer(k)],
-            dst_ref=relay.at[b, p],
+            dst_ref=relay.at[b, p, i],
             send_sem=p_ss.at[b, p, k - 1],
-            recv_sem=r_rs.at[b, p],
+            recv_sem=r_rs.at[b, p, i],
             device_id={"dp": jnp.where(d == 0, 1, n_dp - 2)},
             device_id_type=MESH_ID,
         )
 
-    def pack(sq):
-        hi = sq.astype(bf16).astype(f32)
-        return jnp.where(lane == 0, hi, jnp.where(lane == 1, sq - hi, 0.0)).astype(bf16)
-
-    def send_step(b, p, i):
-        k = offset(i)
-        c = partial_copy(b, p, k)
-        if relayed and i == 0:
-
-            @pl.when(at_end)
+    def square_copy(b, p, k):
+        return pltpu.make_async_remote_copy(
+            src_ref=sqx.at[b, p, d],
+            dst_ref=sqx.at[b, p, d],
+            send_sem=q_ss.at[b, p, k - 1],
+            recv_sem=q_rs.at[b, p, k - 1],
+            device_id={"dp": dp_peer(k)},
+            device_id_type=MESH_ID,
+        )
+
+    def far_along(i):
+        middle = far_first(n_dp)[i]
+        return jnp.where(d == 0, n_dp - 1 - i, jnp.where(d == n_dp - 1, i + 1, middle))
+
+    def send_partials(b, p):
+        for k in range(1, n_dp):
+            sends.append(partial_copy(b, p, k))
+        if not relayed:
+            for k in far_first(n_dp):
+                partial_copy(b, p, k).start()
+            return
+
+        @pl.when(at_end)
+        def _():
+            for i in range(n_dp - 2):
+                k = jnp.where(d == 0, n_dp - 1 - i, i + 1)
+                c = relay_copy(b, p, k, i) if i < hops else partial_copy(b, p, k)
+                c.start()
+
+        @pl.when(merging)
+        def _():
+            for i in range(n_dp - 1 - hops):
+                k = jnp.where(d == 1, i, n_dp - i) if i else jnp.where(d == 1, n_dp - 1, 1)
+                partial_copy(b, p, k).start()
+
+        if n_dp > 4:
+
+            @pl.when(jnp.logical_not(jnp.logical_or(at_end, merging)))
             def _():
-                relay_copy(b, p, k).start()
-
-            @pl.when(jnp.logical_not(at_end))
-            def _():
-                c.start()
-
-        else:
-            if relayed and i == last:
-
-                @pl.when(merging)
-                def _():
-                    relay_copy(b, p, k).wait_recv()
-                    dest = dp_peer(k)
-                    for j in range(4):
-                        cols = slice(j * chans, (j + 1) * chans)
-                        both = pf[p, dest, :, cols] + relay[b, p, :, cols].astype(f32)
-                        psend[b, p, dest, :, cols] = both.astype(bf16)
-                    far = jnp.sum(relay[b, p, :, 4 * chans :].astype(f32), axis=1, keepdims=True)
-                    psend[b, p, dest, :, 4 * chans :] = pack(sq_s[p, dest] + far)
-
-            c.start()
-        sends.append(c)
+                for k in far_first(n_dp):
+                    partial_copy(b, p, k).start()
+
+    def finish_ends(b, p):
+        if relayed:
+            pl.when(at_end)(partial_copy(b, p, jnp.where(d == 0, 1, n_dp - 1)).start)
+
+    def merge(b, p, i):
+        @pl.when(merging)
+        def _():
+            dest = jnp.where(d == 1, n_dp - 1 - i, i)
+            k = lax.rem(dest - d + n_dp, n_dp)
+            relay_copy(b, p, k, i).wait_recv()
+            for j in range(4):
+                cols = slice(j * chans, (j + 1) * chans)
+                both = pf[p, dest, :, cols] + relay[b, p, i, :, cols].astype(f32)
+                psend[b, p, dest, :, cols] = both.astype(bf16)
+            partial_copy(b, p, k).start()
+
+    def merge_far(b, p):
+        if relayed:
+            merge(b, p, 0)
+
+    def merge_near(b, p):
+        if relayed:
+            for i in range(1, hops):
+                merge(b, p, i)
+
+    def bypassed(k):
+        source = lax.rem(d - k + n_dp, n_dp)
+        low = jnp.logical_and(source == 0, d >= n_dp - hops)
+        return jnp.logical_or(low, jnp.logical_and(source == n_dp - 1, d < hops))
 
     def project(b, p):
         if p == 0:
             for i in range(4):
                 loads[b][i].wait()
-        for k in range(1, n_tp):
-            x_copy(b, p, k).wait_recv()
+        if b == 0:
+            for k in range(1, n_tp):
+                x_copy(b, p, k).wait_recv()
         x = xall[b, p].reshape(rows_all, feats).astype(f32)
         sq = jnp.sum(x * x, axis=1, keepdims=True)
         gained = (x * gain_s[b : b + 1, :].astype(f32)).astype(bf16)
-        sq_s[p] = jnp.broadcast_to(sq, (rows_all, 128)).reshape(n_dp, hr, 128)
-        for e in range(n_dp):
-            psend[b, p, e, :, 4 * chans :] = pack(jnp.broadcast_to(sq[e * hr : (e + 1) * hr], (hr, 128)))
+        square = lax.broadcasted_iota(jnp.int32, (rows_all, rows_all), 0) == lax.broadcasted_iota(
+            jnp.int32, (rows_all, rows_all), 1
+        )
+        sqx[b, p, d] = jnp.sum(jnp.where(square, sq, 0.0), axis=0, keepdims=True)
+        for i in range(n_dp - 1):
+            c = square_copy(b, p, far_along(i))
+            c.start()
+            sends.append(c)
         for i in range(4):
             cols = slice(i * chans, (i + 1) * chans)
             part = jnp.dot(gained, wbuf[b, i], preferred_element_type=f32)
             pf[p, :, :, cols] = part.reshape(n_dp, hr, chans)
             psend[b, p, :, :, cols] = part.astype(bf16).reshape(n_dp, hr, chans)
-        for i in range(last):
-            send_step(b, p, i)
-
-    def finish_sends(b, p):
-        send_step(b, p, last)
+        send_partials(b, p)
 
     def gates(b, p):
         if b == 0 and p == 0:
@@ -250,16 +300,21 @@
                 c.wait()
         for k in range(1, n_dp):
             c = partial_copy(b, p, k)
-            if relayed and k == 1:
-                pl.when(d != 0)(c.wait_recv)
-            elif relayed and k == n_dp - 1:
-                pl.when(d != n_dp - 1)(c.wait_recv)
+            if relayed:
+                pl.when(jnp.logical_not(bypassed(k)))(c.wait_recv)
             else:
                 c.wait_recv()
 
-        squares = sq_s[p, d, :, :1]
-        for k in range(n_dp - 1):
-            squares = squares + jnp.sum(precv[b, p, k, :, 4 * chans :].astype(f32), axis=1, keepdims=True)
+        for k in range(1, n_dp):
+            square_copy(b, p, k).wait_recv()
+        row = sqx[b, p, 0]
+        for e in range(1, n_dp):
+            row = row + sqx[b, p, e]
+        mine = (
+            lax.broadcasted_iota(jnp.int32, (hr, rows_all), 1)
+            == lax.broadcasted_iota(jnp.int32, (hr, rows_all), 0) + d * hr
+        )
+        squares = jnp.sum(jnp.where(mine, row, 0.0), axis=1, keepdims=True)
         scale = lax.rsqrt(squares / width + epsilon)
 
         def total(i):
@@ -309,8 +364,9 @@
             mean = jnp.mean(readout * readout, axis=1, keepdims=True)
             normed = readout * lax.rsqrt(mean + epsilon) * hgain_s[b : b + 1, :] * gate_s[:, cols]
             nall[b, p, d, :, cols] = normed.astype(bf16)
-        for k in far_first(n_dp):
-            c = normed_copy(b, p, k)
+    def share_normed(b, p):
+        for i in range(n_dp - 1):
+            c = normed_copy(b, p, far_along(i))
             c.start()
             sends.append(c)
 
@@ -328,9 +384,9 @@
         dest = tp_peer(k)
         return pltpu.make_async_remote_copy(
             src_ref=osend.at[b, p, dest],
-            dst_ref=orecv.at[b, p, k - 1],
-            send_sem=o_ss.at[b, p, k - 1],
-            recv_sem=o_rs.at[b, p, k - 1],
+            dst_ref=orecv.at[p, k - 1],
+            send_sem=o_ss.at[p, k - 1],
+            recv_sem=o_rs.at[p, k - 1],
             device_id={"tp": dest},
             device_id_type=MESH_ID,
         )
@@ -344,23 +400,74 @@
         part = jnp.dot(rows, wobuf[b], preferred_element_type=f32)
         po[p] = part.reshape(n_tp, rh, feats)
         osend[b, p] = part.astype(bf16).reshape(n_tp, rh, feats)
+        if b == 0:
+            c = pair_copy(p)
+            c.start()
+            sends.append(c)
+            return
         for k in far_first(n_tp):
             c = out_copy(b, p, k)
             c.start()
             sends.append(c)
 
+    def pair_copy(p):
+        return pltpu.make_async_remote_copy(
+            src_ref=osend.at[0, p],
+            dst_ref=pair.at[p],
+            send_sem=d_ss.at[p],
+            recv_sem=d_rs.at[p],
+            device_id={"tp": t + 1 - 2 * core},
+            device_id_type=MESH_ID,
+        )
+
+    def cross_copy(p, i):
+        return pltpu.make_async_remote_copy(
+            src_ref=zsend.at[p],
+            dst_ref=zrecv.at[p, i // 2, core],
+            send_sem=z_ss.at[p, i],
+            recv_sem=z_rs.at[p, i // 2, core],
+            device_id={"tp": lax.rem(2 * chip + i + 2, n_tp)},
+            device_id_type=MESH_ID,
+        )
+
+    def cross_wait(p, i, c):
+        arrived = pltpu.make_async_remote_copy(
+            src_ref=zsend.at[p],
+            dst_ref=zrecv.at[p, i, c],
+            send_sem=z_ss.at[p, i],
+            recv_sem=z_rs.at[p, i, c],
+            device_id={"tp": lax.rem(t + 1, n_tp)},
+            device_id_type=MESH_ID,
+        )
+        arrived.wait_recv()
+
+    def cross(b, p):
+        if b == 1:
+            return
+        pair_copy(p).wait_recv()
+        po[p] = po[p] + pair[p].astype(f32)
+        zsend[p] = po[p, pl.ds(core * chips, chips)].astype(bf16)
+        for i in range(n_tp - 2):
+            c = cross_copy(p, i)
+            c.start()
+            sends.append(c)
+
     def residual(b, p):
+        if b == 0:
+            for c in range(2):
+                half = slice(c * chips, (c + 1) * chips)
+                branch = po[p, half]
+                for i in range(chips - 1):
+                    cross_wait(p, i, c)
+                    branch = branch + zrecv[p, i, c].astype(f32)
+                xall[1, p, half] = (xall[0, p, half].astype(f32) + branch).astype(bf16)
+            return
         for k in range(1, n_tp):
             out_copy(b, p, k).wait_recv()
         branch = po[p, t]
         for k in range(n_tp - 1):
-            branch = branch + orecv[b, p, k].astype(f32)
-        result = xall[b, p, t].astype(f32) + branch
-        if b == 0:
-            xall[1, p, t] = result.astype(bf16)
-            share(1, p)
-        else:
-            mixed[p * rh : (p + 1) * rh, :] = result
+            branch = branch + orecv[p, k].astype(f32)
+        mixed[p * rh : (p + 1) * rh, :] = xall[b, p, t].astype(f32) + branch
 
     def advance(b, p):
         def step(g, carry):
@@ -391,9 +498,9 @@
         lax.fori_loop(0, per_part, step, 0)
 
     if relayed:
-        for k, end in ((1, 0), (n_dp - 1, n_dp - 1)):
-
-            @pl.when(d == end)
+        for k in range(1, n_dp):
+
+            @pl.when(bypassed(k))
             def _():
                 for b in range(2):
                     for p in range(parts):
@@ -410,37 +517,23 @@
     small[0].wait()
 
     if parts == 1:
-        order = []
-        for b in range(2):
-            order += [(f, b, 0) for f in (project, finish_sends, gates, advance, out_project, residual)]
+        order = [(f, k) for k in range(2) for f in "PEMNGAVOZY"]
     else:
-        order = [
-            (project, 0, 0),
-            (finish_sends, 0, 0),
-            (project, 0, 1),
-            (gates, 0, 0),
-            (finish_sends, 0, 1),
-            (advance, 0, 0),
-            (out_project, 0, 0),
-            (gates, 0, 1),
-            (residual, 0, 0),
-            (project, 1, 0),
-            (advance, 0, 1),
-            (out_project, 0, 1),
-            (finish_sends, 1, 0),
-            (residual, 0, 1),
-            (project, 1, 1),
-            (gates, 1, 0),
-            (finish_sends, 1, 1),
-            (advance, 1, 0),
-            (out_project, 1, 0),
-            (gates, 1, 1),
-            (residual, 1, 0),
-            (advance, 1, 1),
-            (out_project, 1, 1),
-            (residual, 1, 1),
-        ]
-    for f, b, p in order:
+        order = [(step[0], int(step[1:])) for step in ORDER]
+    stages = dict(
+        P=project,
+        E=finish_ends,
+        M=merge_far,
+        N=merge_near,
+        G=gates,
+        A=share_normed,
+        O=out_project,
+        Z=cross,
+        Y=residual,
+        V=advance,
+    )
+    for name, k in order:
+        f, b, p = stages[name], k // parts, k % parts
         f(b, p)
 
     for c in sends:
@@ -464,9 +557,9 @@
     rt, feats = tokens.shape
     own, heads, size = state.shape[1:4]
     chans = heads * size
-    parts = 2 if own == rt and own % (4 * GROUP) == 0 else 1
+    parts = PARTS if own == rt and own % (2 * GROUP * PARTS) == 0 else 1
     hr, rh = own // parts, rt // parts
-    msg = 4 * chans + 128
+    msg = 4 * chans
     vmem = pl.BlockSpec(memory_space=pltpu.VMEM)
     hbm = pl.BlockSpec(memory_space=pl.ANY)
     dma = pltpu.SemaphoreType.DMA
@@ -488,14 +581,17 @@
             pltpu.VMEM((2, 4, feats, chans), bf16),
             pltpu.VMEM((2, chans, feats), bf16),
             pltpu.VMEM((parts, n_dp, hr, 4 * chans), f32),
-            pltpu.VMEM((parts, n_dp, hr, 128), f32),
+            pltpu.VMEM((2, parts, n_dp, 1, n_dp * hr), f32),
             pltpu.VMEM((2, parts, n_dp, hr, msg), bf16),
             pltpu.VMEM((2, parts, n_dp - 1, hr, msg), bf16),
-            pltpu.VMEM((2, parts, hr, msg), bf16),
+            pltpu.VMEM((2, parts, max(n_dp - 2, 1), hr, msg), bf16),
             pltpu.VMEM((2, parts, n_dp, hr, chans), bf16),
             pltpu.VMEM((parts, n_tp, rh, feats), f32),
             pltpu.VMEM((2, parts, n_tp, rh, feats), bf16),
-            pltpu.VMEM((2, parts, n_tp - 1, rh, feats), bf16),
+            pltpu.VMEM((parts, n_tp - 1, rh, feats), bf16),
+            pltpu.VMEM((parts, n_tp, rh, feats), bf16),
+            pltpu.VMEM((parts, n_tp // 2, rh, feats), bf16),
+            pltpu.VMEM((parts, n_tp // 2 - 1, 2, n_tp // 2, rh, feats), bf16),
             pltpu.VMEM((hr, chans), f32),
             pltpu.VMEM((hr, chans), f32),
             pltpu.VMEM((hr, chans), f32),
@@ -508,11 +604,17 @@
             dma((2, parts, n_tp - 1)),
             dma((2, parts, n_dp - 1)),
             dma((2, parts, n_dp - 1)),
-            dma((2, parts)),
+            dma((2, parts, max(n_dp - 2, 1))),
             dma((2, parts, n_dp - 1)),
             dma((2, parts, n_dp - 1)),
-            dma((2, parts, n_tp - 1)),
-            dma((2, parts, n_tp - 1)),
+            dma((2, parts, n_dp - 1)),
+            dma((2, parts, n_dp - 1)),
+            dma((parts, n_tp - 1)),
+            dma((parts, n_tp - 1)),
+            dma((parts,)),
+            dma((parts,)),
+            dma((parts, n_tp - 2)),
+            dma((parts, n_tp // 2 - 1, 2)),
         ],
         compiler_params=pltpu.CompilerParams(
             collective_id=0, has_side_effects=True, vmem_limit_bytes=LIMIT

time: 83.7 us -> 75.3 us (0.90)
  Pallas kernels: 82.9 us -> 74.5 us
    pallas_call x1, Pallas kernels: 71.8 us -> 63.3 us  [shards(): pl.pallas_call(functools.partial(chain, n_tp, n_dp, feats * n_dp, parts),...]
where the time goes in v2:
time: 75.3 us; the launch traced here: 75.1 us
  Pallas kernels  74.5 us (99%)
    pallas_call x1, Pallas kernels, shards(): pl.pallas_call(functools.partial(chain, n_tp, n_dp, feats * n_dp, parts),...  63.3 us
    pallas_call x1, Pallas kernels, shards(): pl.pallas_call(store, name='store', out_shape=(jax.ShapeDtypeStruct((rt,...  11.2 us

profile of v2, /device:TPU:0, one launch (start us, length us, event | category | flops | bytes accessed | tf_op | source)
XLA Modules:
  0.0 75.1 jit_solution(3523289998348103509)
XLA Ops:
  0.6 63.3 %chain.1 = (f32[64,512]{1,0:T(8,128)S(1)}, f32[2,64,4,128,128]{4,3,2,1,0:T(8,128)S(1)}) custom-call(bf16[64,512]{1,0:T(8,128)(2,1)} %tokens.1, f32[2,64,4,128,128]{4,3,2,1,0:T(8,128)} %state.1, s32[1,64]{1,0:T(1,128)} %bitcast.1, bf16[2,512]{1,0:T(2,128)(2,1)} %gain.1, bf16[2,512,512]{2,1,0:T(8,128)(2,1)} %w_query.1, bf16[2,512,512]{2,1,0:T(8,128)(2,1)} %w_forget.1, ...), custom_call_target="tpu_custom_call" | custom-call | tf_op jit(solution)/shard_map/chain/pallas_call | solution.py:566
  64.0 11.2 %store.1 = (f32[64,512]{1,0:T(8,128)}, f32[2,64,4,128,128]{4,3,2,1,0:T(8,128)}) custom-call(f32[64,512]{1,0:T(8,128)S(1)} %get-tuple-element.4.mixed, f32[2,64,4,128,128]{4,3,2,1,0:T(8,128)S(1)} %get-tuple-element.5.new_state), custom_call_target="tpu_custom_call" | custom-call | tf_op jit(solution)/shard_map/store/pallas_call | solution.py:624

commit v3 on v2

--- a/solution.py
+++ b/solution.py
@@ -12,6 +12,7 @@
 GROUP = 8
 PARTS = 4
 RELAYS = 2
+EARLY = 3
 LIMIT = 26 * 1024 * 1024
 MESH_ID = pl.DeviceIdType.MESH
 f32 = jnp.float32
@@ -19,11 +20,11 @@
 
 
 ORDER = (
-    "P0", "P1", "E0", "E1", "M0", "N0", "M1", "N1", "G0", "A0", "P2", "G1", "A1", "P3", "E2", "E3", "O0",
-    "M2", "N2", "M3", "Z0", "N3", "G2", "A2", "O1", "Y0", "P4", "Z1", "G3", "A3", "V3", "O2", "E4", "Y1",
-    "P5", "M4", "E5", "Z2", "O3", "M5", "Z3", "Y2", "N4", "N5", "P6", "Y3", "P7", "E6", "M6", "E7", "N6",
-    "G5", "M7", "V2", "N7", "V1", "G4", "A4", "V0", "A5", "G6", "A6", "G7", "A7", "O4", "O5", "V4", "O6",
-    "O7", "V6", "Y4", "V5", "V7", "Y6", "Y5", "Y7",
+    "P0", "P1", "E0", "M0", "E1", "N0", "M1", "N1", "G0", "A0", "P2", "G1", "A1", "P3", "O0", "E2", "M2",
+    "Z0", "N2", "E3", "M3", "N3", "G2", "A2", "O1", "Y0", "P4", "Z1", "G3", "A3", "E4", "O2", "Y1", "P5",
+    "E5", "M4", "N4", "Z2", "O3", "Z3", "Y2", "P6", "M5", "V1", "N5", "Y3", "P7", "G4", "E6", "E7", "M6",
+    "N6", "M7", "N7", "G5", "A4", "G6", "A5", "V3", "A6", "G7", "A7", "V0", "O5", "O4", "O6", "O7", "Y5",
+    "V2", "Y6", "Y4", "Y7",
 )
 
 
@@ -46,6 +47,8 @@
     head_gain,
     mixed,
     sbuf,
+    late_forget,
+    late_value,
     lengths_s,
     gain_s,
     bound_s,
@@ -100,6 +103,7 @@
     rows_all = n_dp * hr
     per_part = hr // GROUP
     relayed = n_dp >= 4
+    early = min(EARLY, parts) if n_dp == 4 and parts > 1 else 0
     hops = min(RELAYS, n_dp - 2)
     core, chip, chips = lax.rem(t, 2), lax.div(t, 2), n_tp // 2
     at_end = jnp.logical_or(d == 0, d == n_dp - 1)
@@ -147,15 +151,9 @@
         pl.semaphore_signal(barrier, inc=1, device_id={"dp": dp_peer(k)}, device_id_type=MESH_ID)
     pl.semaphore_wait(barrier, n_tp + n_dp - 2)
 
-    sends = []
+    sends, ready = [], []
     row_id = lax.broadcasted_iota(jnp.int32, (GROUP, size), 0)
-    spread = jnp.where(
-        lax.broadcasted_iota(jnp.int32, (GROUP, GROUP * size), 1) // size
-        == lax.broadcasted_iota(jnp.int32, (GROUP, GROUP * size), 0),
-        1.0,
-        0.0,
-    ).astype(bf16)
-    spread = jnp.concatenate([spread] * 3, axis=0)
+    spread = spreader(size)
 
     def far_first(n):
         return [n // 2] + [k for k in range(1, n) if k != n // 2]
@@ -224,13 +222,13 @@
             for i in range(n_dp - 2):
                 k = jnp.where(d == 0, n_dp - 1 - i, i + 1)
                 c = relay_copy(b, p, k, i) if i < hops else partial_copy(b, p, k)
-                c.start()
+                unless_early(b, p, k, c)
 
         @pl.when(merging)
         def _():
             for i in range(n_dp - 1 - hops):
                 k = jnp.where(d == 1, i, n_dp - i) if i else jnp.where(d == 1, n_dp - 1, 1)
-                partial_copy(b, p, k).start()
+                unless_early(b, p, k, partial_copy(b, p, k))
 
         if n_dp > 4:
 
@@ -241,7 +239,47 @@
 
     def finish_ends(b, p):
         if relayed:
-            pl.when(at_end)(partial_copy(b, p, jnp.where(d == 0, 1, n_dp - 1)).start)
+
+            @pl.when(at_end)
+            def _():
+                k = jnp.where(d == 0, 1, n_dp - 1)
+                unless_early(b, p, k, partial_copy(b, p, k))
+
+    def unless_early(b, p, k, c):
+        if b == 0 and p < early:
+            pl.when(dp_peer(k) != t)(c.start)
+        else:
+            c.start()
+
+    def send_early():
+        for i in range(4):
+            loads[0][i].wait()
+        x = jnp.concatenate([xall[0, p, t] for p in range(early)], axis=0).astype(f32)
+        gained = (x * gain_s[:1, :].astype(f32)).astype(bf16)
+        for i in range(4):
+            cols = slice(i * chans, (i + 1) * chans)
+            part = jnp.dot(gained, wbuf[0, i], preferred_element_type=f32)
+            for p in range(early):
+                mine = part[p * hr : (p + 1) * hr]
+                pf[p, t, :, cols] = mine
+                psend[0, p, t, :, cols] = mine.astype(bf16)
+        k = lax.rem(t - d + n_dp, n_dp)
+
+        @pl.when(jnp.logical_and(at_end, t != d))
+        def _():
+            slot = jnp.where(d == 0, n_dp - 1 - t, t)
+            for p in range(early):
+
+                @pl.when(slot < hops)
+                def _():
+                    relay_copy(0, p, k, slot).start()
+
+                pl.when(slot >= hops)(partial_copy(0, p, k).start)
+
+        @pl.when(jnp.logical_and(merging, t == jnp.where(d == 1, 0, n_dp - 1)))
+        def _():
+            for p in range(early):
+                partial_copy(0, p, k).start()
 
     def merge(b, p, i):
         @pl.when(merging)
@@ -270,7 +308,7 @@
         return jnp.logical_or(low, jnp.logical_and(source == n_dp - 1, d < hops))
 
     def project(b, p):
-        if p == 0:
+        if p == 0 and not (b == 0 and early):
             for i in range(4):
                 loads[b][i].wait()
         if b == 0:
@@ -291,7 +329,15 @@
             cols = slice(i * chans, (i + 1) * chans)
             part = jnp.dot(gained, wbuf[b, i], preferred_element_type=f32)
             pf[p, :, :, cols] = part.reshape(n_dp, hr, chans)
-            psend[b, p, :, :, cols] = part.astype(bf16).reshape(n_dp, hr, chans)
+            if b == 1 or p >= early:
+                psend[b, p, :, :, cols] = part.astype(bf16).reshape(n_dp, hr, chans)
+        if b == 0 and p < early:
+            for e in range(n_dp):
+
+                @pl.when(t != e)
+                def _():
+                    psend[0, p, e] = pf[p, e].astype(bf16)
+
         send_partials(b, p)
 
     def gates(b, p):
@@ -332,11 +378,15 @@
         pre = total(1) - pace_s[b : b + 1, :] * log_len
         forget = lower + (1.0 - lower) * jax.nn.sigmoid(pre)
         key = (1.0 - lower) * jax.nn.sigmoid(-pre)
-        forget_s[b, rows] = forget
+        if b == 0:
+            forget_s[rows] = forget
+        else:
+            late_forget[rows] = forget
         query = total(0)
         qf_s[...] = query * forget
         qk_s[...] = query * key
-        value_s[b, rows] = total(2)
+        value = value_s if b == 0 else late_value
+        value[rows] = total(2)
         gate = total(3)
         gate_s[...] = gate * jax.nn.sigmoid(gate)
 
@@ -360,7 +410,7 @@
         for h in range(heads):
             cols = slice(h * size, (h + 1) * size)
             dots = jnp.sum(qk_s[:, cols], axis=1, keepdims=True)
-            readout = ro_s[:, cols] + dots * value_s[b, rows, cols]
+            readout = ro_s[:, cols] + dots * value[rows, cols]
             mean = jnp.mean(readout * readout, axis=1, keepdims=True)
             normed = readout * lax.rsqrt(mean + epsilon) * hgain_s[b : b + 1, :] * gate_s[:, cols]
             nall[b, p, d, :, cols] = normed.astype(bf16)
@@ -392,7 +442,8 @@
         )
 
     def out_project(b, p):
-        if p == 0:
+        if b not in ready:
+            ready.append(b)
             loads[b][4].wait()
         for k in range(1, n_dp):
             normed_copy(b, p, k).wait_recv()
@@ -473,29 +524,15 @@
         def step(g, carry):
             base = pl.multiple_of(p * hr + g * GROUP, GROUP)
             rows = pl.ds(base, GROUP)
-            f = forget_s[b, rows, :]
-            top = f.astype(bf16)
-            rest = f - top.astype(f32)
-            mid = rest.astype(bf16)
-            low = (rest - mid.astype(f32)).astype(bf16)
-            pieces = jnp.concatenate([top, mid, low], axis=0)
-            for h in range(heads):
-                cols = slice(h * size, (h + 1) * size)
-                v = value_s[b, rows, cols]
-                for j in range(0, GROUP, 2):
-                    wide = lax.dot_general(
-                        pieces[:, cols],
-                        spread[:, j * size : (j + 2) * size],
-                        (((0,), (0,)), ((), ())),
-                        preferred_element_type=f32,
-                    )
-                    for i in range(2):
-                        row = v[j + i : j + i + 1, :]
-                        keep = wide[:, i * size : (i + 1) * size]
-                        sbuf[b, base + j + i, h] = row + keep * (sbuf[b, base + j + i, h] - row)
+
+            def write(j, h, new):
+                sbuf[0, base + j, h] = new
+
+            update(lambda j, h: sbuf[0, base + j, h], write, heads, forget_s[rows, :], value_s[rows, :], spread)
             return carry
 
-        lax.fori_loop(0, per_part, step, 0)
+        if b == 0:
+            lax.fori_loop(0, per_part, step, 0)
 
     if relayed:
         for k in range(1, n_dp):
@@ -515,6 +552,8 @@
     for g in range(own // GROUP):
         state_load(1, g).start()
     small[0].wait()
+    if early:
+        send_early()
 
     if parts == 1:
         order = [(f, k) for k in range(2) for f in "PEMNGAVOZY"]
@@ -540,17 +579,69 @@
         c.wait_send()
 
 
-def store(mixed, new_state, mixed_out, state_out, sems):
-    blocks, own = new_state.shape[:2]
-    copies = [pltpu.make_async_copy(mixed, mixed_out, sems.at[blocks, 0])]
-    for b in range(blocks):
-        for g in range(own // GROUP):
-            rows = pl.ds(g * GROUP, GROUP)
-            copies.append(pltpu.make_async_copy(new_state.at[b, rows], state_out.at[b, rows], sems.at[b, g]))
-    for c in copies:
-        c.start()
-    for c in copies:
-        c.wait()
+def spreader(size):
+    lane = lax.broadcasted_iota(jnp.int32, (GROUP, GROUP * size), 1)
+    row = lax.broadcasted_iota(jnp.int32, (GROUP, GROUP * size), 0)
+    ones = jnp.where(lane // size == row, 1.0, 0.0).astype(bf16)
+    return jnp.concatenate([ones] * 3, axis=0)
+
+
+def update(read, write, heads, forget, value, spread):
+    size = value.shape[1] // heads
+    top = forget.astype(bf16)
+    rest = forget - top.astype(f32)
+    mid = rest.astype(bf16)
+    low = (rest - mid.astype(f32)).astype(bf16)
+    pieces = jnp.concatenate([top, mid, low], axis=0)
+    for h in range(heads):
+        cols = slice(h * size, (h + 1) * size)
+        for j in range(0, GROUP, 2):
+            wide = lax.dot_general(
+                pieces[:, cols],
+                spread[:, j * size : (j + 2) * size],
+                (((0,), (0,)), ((), ())),
+                preferred_element_type=f32,
+            )
+            for i in range(2):
+                row = value[j + i : j + i + 1, cols]
+                keep = wide[:, i * size : (i + 1) * size]
+                write(j + i, h, row + keep * (read(j + i, h) - row))
+
+
+def store(mixed, new_state, forget, value, mixed_out, state_out, fresh, sems):
+    own, heads, size = new_state.shape[1:4]
+    groups = own // GROUP
+
+    def early(g):
+        rows = pl.ds(g * GROUP, GROUP)
+        return pltpu.make_async_copy(new_state.at[0, rows], state_out.at[0, rows], sems.at[0, g])
+
+    def late(g):
+        rows = pl.ds(g * GROUP, GROUP)
+        return pltpu.make_async_copy(fresh.at[rows], state_out.at[1, rows], sems.at[1, g])
+
+    rest = pltpu.make_async_copy(mixed, mixed_out, sems.at[2, 0])
+    rest.start()
+    for g in range(groups):
+        early(g).start()
+    spread = spreader(size)
+
+    def step(g, carry):
+        base = pl.multiple_of(g * GROUP, GROUP)
+        rows = pl.ds(base, GROUP)
+
+        def write(j, h, new):
+            fresh[base + j, h] = new
+
+        update(lambda j, h: new_state[1, base + j, h], write, heads, forget[rows, :], value[rows, :], spread)
+        late(g).start()
+        return carry
+
+    lax.fori_loop(0, groups, step, 0)
+    rest.wait()
+    for g in range(groups):
+        early(g).wait()
+        late(g).wait()
 
 
 def shards(n_tp, n_dp, tokens, state, lengths, gain, w_query, w_forget, w_input, w_gate, w_out, bound, pace, head_gain):
@@ -563,20 +654,21 @@
     vmem = pl.BlockSpec(memory_space=pltpu.VMEM)
     hbm = pl.BlockSpec(memory_space=pl.ANY)
     dma = pltpu.SemaphoreType.DMA
-    mixed, new_state = pl.pallas_call(
+    late = pltpu.VMEM((own, chans), f32)
+    outputs = pl.pallas_call(
         functools.partial(chain, n_tp, n_dp, feats * n_dp, parts),
         name="chain",
-        out_shape=(pltpu.VMEM((rt, feats), f32), pltpu.VMEM(state.shape, f32)),
+        out_shape=(pltpu.VMEM((rt, feats), f32), pltpu.VMEM(state.shape, f32), late, late),
         in_specs=[hbm] * 12,
-        out_specs=(vmem, vmem),
+        out_specs=(vmem,) * 4,
         scratch_shapes=[
             pltpu.VMEM((1, own), jnp.int32),
             pltpu.VMEM(gain.shape, bf16),
             pltpu.VMEM(bound.shape, f32),
             pltpu.VMEM(pace.shape, f32),
             pltpu.VMEM(head_gain.shape, f32),
-            pltpu.VMEM((2, own, chans), f32),
-            pltpu.VMEM((2, own, chans), f32),
+            pltpu.VMEM((own, chans), f32),
+            pltpu.VMEM((own, chans), f32),
             pltpu.VMEM((2, parts, n_tp, rh, feats), bf16),
             pltpu.VMEM((2, 4, feats, chans), bf16),
             pltpu.VMEM((2, chans, feats), bf16),
@@ -625,11 +717,11 @@
         store,
         name="store",
         out_shape=(jax.ShapeDtypeStruct((rt, feats), f32), jax.ShapeDtypeStruct(state.shape, f32)),
-        in_specs=[vmem, vmem],
+        in_specs=[vmem] * 4,
         out_specs=(hbm, hbm),
-        scratch_shapes=[dma((3, own // GROUP))],
+        scratch_shapes=[pltpu.VMEM(state.shape[1:], f32), dma((3, own // GROUP))],
         compiler_params=pltpu.CompilerParams(vmem_limit_bytes=LIMIT),
-    )(pltpu.with_memory_space_constraint(mixed, pltpu.VMEM), pltpu.with_memory_space_constraint(new_state, pltpu.VMEM))
+    )(*(pltpu.with_memory_space_constraint(x, pltpu.VMEM) for x in outputs))
 
 
 def solution(mesh):

time: 75.3 us -> 73.4 us (0.975)
  Pallas kernels: 74.5 us -> 72.6 us
    pallas_call x1, Pallas kernels: 63.3 us -> 61.5 us  [shards(): pl.pallas_call(functools.partial(chain, n_tp, n_dp, feats * n_dp, parts),...]
where the time goes in v3:
time: 73.4 us; the launch traced here: 73.3 us
  Pallas kernels  72.6 us (99%)
    pallas_call x1, Pallas kernels, shards(): pl.pallas_call(functools.partial(chain, n_tp, n_dp, feats * n_dp, parts),...  61.5 us
    pallas_call x1, Pallas kernels, shards(): pl.pallas_call(store, name='store', out_shape=(jax.ShapeDtypeStruct((rt,...  11.2 us

profile of v3, /device:TPU:0, one launch (start us, length us, event | category | flops | bytes accessed | tf_op | source)
XLA Modules:
  0.0 73.3 jit_solution(6335997709412580064)
XLA Ops:
  0.6 61.5 %chain.1 = (f32[64,512]{1,0:T(8,128)S(1)}, f32[2,64,4,128,128]{4,3,2,1,0:T(8,128)S(1)}, f32[64,512]{1,0:T(8,128)S(1)}, f32[64,512]{1,0:T(8,128)S(1)}) custom-call(bf16[64,512]{1,0:T(8,128)(2,1)} %tokens.1, f32[2,64,4,128,128]{4,3,2,1,0:T(8,128)} %state.1, s32[1,64]{1,0:T(1,128)} %bitcast.1, bf16[2,512]{1,0:T(2,128)(2,1)} %gain.1, ...), custom_call_target="tpu_custom_call" | custom-call | tf_op jit(solution)/shard_map/chain/pallas_call | solution.py:658
  62.1 11.2 %store.1 = (f32[64,512]{1,0:T(8,128)}, f32[2,64,4,128,128]{4,3,2,1,0:T(8,128)}) custom-call(f32[64,512]{1,0:T(8,128)S(1)} %get-tuple-element.6.mixed, f32[2,64,4,128,128]{4,3,2,1,0:T(8,128)S(1)} %get-tuple-element.7.new_state, f32[64,512]{1,0:T(8,128)S(1)} %get-tuple-element.8.forget, f32[64,512]{1,0:T(8,128)S(1)} %get-tuple-element.9.value), custom_call_target="tpu_custom_call" | custom-call | tf_op jit(solution)/shard_map/store/pallas_call | solution.py:716
